TPU v7x, 32 devices: a whole 2x2x4 slice. The times are simulated.
32 devices in a mesh: grp: 2 (over x), sp: 4 (over y, core), tp: 4 (over z).
Axes of the slice: x: 2, y: 2, z: 4, core: 2. Of those that a mesh axis runs over, the one named last changes fastest.
Arguments:
- tokens_in: bfloat16 [2048, 2048], P(('grp', 'sp'), 'tp'), parts along dimension 0, may hold values from -8 to 8
- out_gate: bfloat16 [3, 2048, 2048], P(None, 'sp', 'tp'), may hold values from -0.125 to 0.125
- in_gate: bfloat16 [3, 2048, 2048], P(None, 'sp', 'tp'), may hold values from -0.125 to 0.125
- value_proj: bfloat16 [3, 2048, 2048], P(None, 'sp', 'tp'), may hold values from -0.125 to 0.125
- mix_proj: bfloat16 [3, 2048, 2048], P(None, 'sp', 'tp'), may hold values from -0.125 to 0.125
- conv_taps: float32 [3, 3, 2048], P(None, None, 'tp'), may hold values from -3.5 to 3.5
- norm_gains: float32 [3, 2048], P(None, 'tp'), may hold values from 0.1 to 1.9
- final_gain: float32 [2048], P('tp'), may hold values from 0.1 to 1.9
Outputs:
- normed_out: bfloat16 [2048, 2048], P(('grp', 'sp'), 'tp'), parts along dimension 0
There are 2 independent parts, one for each index of `grp`. A program takes and returns all parts, laid end to end along the dimension named above; an argument that names none is the same for every part. Nothing has to cross between parts.
All inputs are finite; a program needn't handle non-finite values.
Results may differ from a plain program's by a relative error of at most 0.025.
Values may be sent and summed in bfloat16 or wider, within the bound.
A program may use at most 64 MiB of HBM per device.

v0:
```python
import jax
import jax.numpy as jnp
from jax import lax
from jax.sharding import PartitionSpec as P

D = 2048
TAPS = 3
LAYERS = 3
epsilon = 1e-06


def passed_along(shard, axis, by):
    peers = lax.axis_size(axis)
    pairs = [(i, i + by) for i in range(peers) if 0 <= i + by < peers]
    return lax.ppermute(shard, axis, pairs)


def row_scale(stream):
    squares = lax.psum(jnp.sum(stream * stream, axis=1, keepdims=True), "tp")
    return lax.rsqrt(squares / D + epsilon)


def shards(tokens_in, out_gate, in_gate, value_proj, mix_proj, conv_taps, norm_gains, final_gain):
    stream = tokens_in.astype(jnp.float32)
    row_count = stream.shape[0]
    reach = TAPS - 1
    whole = (
        lax.all_gather(out_gate, "sp", axis=1, tiled=True),
        lax.all_gather(in_gate, "sp", axis=1, tiled=True),
        lax.all_gather(value_proj, "sp", axis=1, tiled=True),
        lax.all_gather(mix_proj, "sp", axis=1, tiled=True),
    )
    for layer_index in range(LAYERS):
        scale = row_scale(stream)
        normed = (stream * norm_gains[layer_index]).astype(jnp.bfloat16)
        gathered = lax.all_gather(normed, "tp", axis=1, tiled=True)
        products = tuple(
            (
                jnp.dot(gathered, weight[layer_index], preferred_element_type=jnp.float32)
                for weight in whole[:3]
            )
        )
        out_gates, in_gates, values = [
            (product * scale).astype(jnp.bfloat16) for product in products
        ]
        product_v = (in_gates.astype(jnp.float32) * values.astype(jnp.float32)).astype(jnp.bfloat16)
        earlier = passed_along(product_v[row_count - reach :], "sp", 1)
        padded = jnp.concatenate([earlier, product_v], axis=0)
        convolved = padded[0:row_count].astype(jnp.float32) * conv_taps[layer_index, 0]
        for tap_index in range(1, TAPS):
            convolved = (
                convolved
                + padded[tap_index : tap_index + row_count].astype(jnp.float32)
                * conv_taps[layer_index, tap_index]
            )
        gated = (out_gates.astype(jnp.float32) * convolved).astype(jnp.bfloat16)
        spread = lax.all_gather(gated, "tp", axis=1, tiled=True)
        mixed = jnp.dot(spread, whole[3][layer_index], preferred_element_type=jnp.float32)
        stream = stream + mixed
    scale = row_scale(stream)
    return (stream * scale * final_gain).astype(jnp.bfloat16)


def solution(mesh):
    in_specs = (
        P(("grp", "sp"), "tp"),
        P(None, "sp", "tp"),
        P(None, "sp", "tp"),
        P(None, "sp", "tp"),
        P(None, "sp", "tp"),
        P(None, None, "tp"),
        P(None, "tp"),
        P("tp"),
    )
    out_specs = P(("grp", "sp"), "tp")
    return jax.shard_map(shards, mesh=mesh, in_specs=in_specs, out_specs=out_specs, check_vma=False)
```

profile of v0, /device:TPU:0, one launch (start us, length us, event | category | flops | bytes accessed | tf_op | source)
XLA Modules:
  0.0 424.5 jit_solution(9574232206159354128)
XLA Ops:
  6.5 0.8 fusion.60
  7.4 1.7 fusion.55
  9.1 0.0 all-gather.11.cloned.1.call-update
  9.1 0.0 all-gather.17.cloned.1.call-start
  9.2 0.7 all-gather.17.cloned.1.call-update
  9.9 0.0 all-gather.15.cloned.1.call-start
  9.9 0.7 all-gather.15.cloned.1.call-update
  10.6 0.0 all-gather.13.cloned.1.call-start
  10.7 0.5 all-gather.13.cloned.1.call-update
  11.2 0.0 all-gather.21.cloned.1.call-start
  11.2 0.5 all-gather.21.cloned.1.call-update
  11.8 0.0 all-gather.19.cloned.1.call-start
  11.8 13.5 %psum.28 = f32[256,1]{0,1:T(1,128)S(1)} all-reduce(f32[256,1]{0,1:T(1,128)S(1)} %bitcast.159), channel_id=1, replica_groups=mesh['grp'=2,'sp'=4,'tp'=4] {'tp'}, use_global_device_ids=true, to_apply=%region_1.0 | all-reduce | flops 256 | bytes 2048 | tf_op jit(solution)/shard_map/psum | solution.py:19
  25.3 14.7 %all-gather.11.cloned.1.call-done = bf16[256,2048]{1,0:T(8,128)(2,1)} async-done(((bf16[256,512]{1,0:T(8,128)(2,1)}), bf16[256,2048]{1,0:T(8,128)(2,1)}) %all-gather.11.cloned.1.call-update) | async-done | bytes 1048592 | tf_op jit(solution)/shard_map/all_gather | solution.py:36
  40.0 47.3 %all-gather.17.cloned.1.call-done = bf16[3,2048,512]{2,1,0:T(8,128)(2,1)} async-done(((bf16[3,512,512]{2,1,0:T(8,128)(2,1)}), bf16[3,2048,512]{2,1,0:T(8,128)(2,1)}) %all-gather.17.cloned.1.call-update) | async-done | bytes 6291472 | tf_op jit(solution)/shard_map/all_gather | solution.py:30
  87.3 2.6 fusion.39
  90.0 45.3 %all-gather.15.cloned.1.call-done = bf16[3,2048,512]{2,1,0:T(8,128)(2,1)} async-done(((bf16[3,512,512]{2,1,0:T(8,128)(2,1)}), bf16[3,2048,512]{2,1,0:T(8,128)(2,1)}) %all-gather.15.cloned.1.call-update) | async-done | bytes 6291472 | tf_op jit(solution)/shard_map/all_gather | solution.py:29
  135.3 2.6 fusion.38
  137.9 2.2 collective-permute-start
  140.1 43.0 %all-gather.13.cloned.1.call-done = bf16[3,2048,512]{2,1,0:T(8,128)(2,1)} async-done(((bf16[3,512,512]{2,1,0:T(8,128)(2,1)}), bf16[3,2048,512]{2,1,0:T(8,128)(2,1)}) %all-gather.13.cloned.1.call-update) | async-done | bytes 6291472 | tf_op jit(solution)/shard_map/all_gather | solution.py:28
  183.1 3.1 fusion.35
  186.2 0.0 all-gather.23.cloned.1.call-start
  186.3 44.6 %all-gather.21.cloned.1.call-done = bf16[3,2048,512]{2,1,0:T(8,128)(2,1)} async-done(((bf16[3,512,512]{2,1,0:T(8,128)(2,1)}), bf16[3,2048,512]{2,1,0:T(8,128)(2,1)}) %all-gather.21.cloned.1.call-update) | async-done | bytes 6291472 | tf_op jit(solution)/shard_map/all_gather | solution.py:31
  230.9 29.4 %all-gather.19.cloned.1.call-done = bf16[256,2048]{1,0:T(8,128)(2,1)} async-done(((bf16[256,512]{1,0:T(8,128)(2,1)}), bf16[256,2048]{1,0:T(8,128)(2,1)}) %all-gather.19.cloned.1.call-update) | async-done | bytes 1048592 | tf_op jit(solution)/shard_map/all_gather | solution.py:57
  260.3 3.4 multiply_reduce_fusion.2
  263.7 0.0 all-gather.25.cloned.1.call-start
  263.8 10.3 %psum.29 = f32[256,1]{0,1:T(1,128)S(1)} all-reduce(f32[256,1]{0,1:T(1,128)S(1)} %bitcast.182), channel_id=1, replica_groups=mesh['grp'=2,'sp'=4,'tp'=4] {'tp'}, use_global_device_ids=true, to_apply=%region_3.0 | all-reduce | flops 256 | bytes 2048 | tf_op jit(solution)/shard_map/psum | solution.py:19
  274.1 17.2 %all-gather.23.cloned.1.call-done = bf16[256,2048]{1,0:T(8,128)(2,1)} async-done(((bf16[256,512]{1,0:T(8,128)(2,1)}), bf16[256,2048]{1,0:T(8,128)(2,1)}) %all-gather.23.cloned.1.call-update) | async-done | bytes 1048592 | tf_op jit(solution)/shard_map/all_gather | solution.py:36
  291.2 2.7 fusion.46
  293.9 2.6 fusion.45
  296.6 1.3 collective-permute-start.1
  297.9 0.8 collective-permute-done.1
  298.7 3.1 fusion.42
  301.8 0.0 all-gather.27.cloned.1.call-start
  301.9 30.3 %all-gather.25.cloned.1.call-done = bf16[256,2048]{1,0:T(8,128)(2,1)} async-done(((bf16[256,512]{1,0:T(8,128)(2,1)}), bf16[256,2048]{1,0:T(8,128)(2,1)}) %all-gather.25.cloned.1.call-update) | async-done | bytes 1048592 | tf_op jit(solution)/shard_map/all_gather | solution.py:57
  332.2 3.3 multiply_reduce_fusion.1
  335.5 0.0 all-gather.29.cloned.1.call-start
  335.6 10.3 %psum.30 = f32[256,1]{0,1:T(1,128)S(1)} all-reduce(f32[256,1]{0,1:T(1,128)S(1)} %bitcast.181), channel_id=1, replica_groups=mesh['grp'=2,'sp'=4,'tp'=4] {'tp'}, use_global_device_ids=true, to_apply=%region_5.0 | all-reduce | flops 256 | bytes 2048 | tf_op jit(solution)/shard_map/psum | solution.py:19
  345.9 17.2 %all-gather.27.cloned.1.call-done = bf16[256,2048]{1,0:T(8,128)(2,1)} async-done(((bf16[256,512]{1,0:T(8,128)(2,1)}), bf16[256,2048]{1,0:T(8,128)(2,1)}) %all-gather.27.cloned.1.call-update) | async-done | bytes 1048592 | tf_op jit(solution)/shard_map/all_gather | solution.py:36
  363.0 2.7 fusion.53
  365.7 2.6 fusion.52
  368.4 1.3 collective-permute-start.2
  369.7 0.8 collective-permute-done.2
  370.5 3.1 fusion.49
  373.6 30.3 %all-gather.29.cloned.1.call-done = bf16[256,2048]{1,0:T(8,128)(2,1)} async-done(((bf16[256,512]{1,0:T(8,128)(2,1)}), bf16[256,2048]{1,0:T(8,128)(2,1)}) %all-gather.29.cloned.1.call-update) | async-done | bytes 1048592 | tf_op jit(solution)/shard_map/all_gather | solution.py:57
  404.0 2.7 multiply_reduce_fusion
  406.7 10.2 %psum.31 = f32[256,1]{0,1:T(1,128)S(1)} all-reduce(f32[256,1]{0,1:T(1,128)S(1)} %bitcast.183), channel_id=1, replica_groups=mesh['grp'=2,'sp'=4,'tp'=4] {'tp'}, use_global_device_ids=true, to_apply=%region_7.0 | all-reduce | flops 256 | bytes 2048 | tf_op jit(solution)/shard_map/psum | solution.py:19
  416.8 0.8 multiply_convert_fusion
  (27 shorter events, 0.2 us)
Async XLA Ops:
  6.5 33.5 %all-gather.11.cloned.1.call-start = ((), (), s32[]{:S(2)}) async-start(), calls=%async_computation | async-start | bytes 1310720 | tf_op jit(solution)/shard_map/all_gather | solution.py:36
  9.1 78.2 %all-gather.17.cloned.1.call-start = ((), (), s32[]{:S(2)}) async-start(), calls=%async_computation.3 | async-start | bytes 7864320 | tf_op jit(solution)/shard_map/all_gather | solution.py:30
  9.9 125.4 %all-gather.15.cloned.1.call-start = ((), (), s32[]{:S(2)}) async-start(), calls=%async_computation.2 | async-start | bytes 7864320 | tf_op jit(solution)/shard_map/all_gather | solution.py:29
  10.6 129.5 %copy-start.1 = (f32[3,3,512]{2,1,0:T(4,128)S(1)}, f32[3,3,512]{2,1,0:T(4,128)}, u32[]{:S(2)}) copy-start(f32[3,3,512]{2,1,0:T(4,128)} %param.13) | copy-start | bytes 55300
  10.6 172.5 %all-gather.13.cloned.1.call-start = ((), (), s32[]{:S(2)}) async-start(), calls=%async_computation.1 | async-start | bytes 7864320 | tf_op jit(solution)/shard_map/all_gather | solution.py:28
  11.2 219.7 %all-gather.21.cloned.1.call-start = ((), (), s32[]{:S(2)}) async-start(), calls=%async_computation.5 | async-start | bytes 7864320 | tf_op jit(solution)/shard_map/all_gather | solution.py:31
  11.8 248.6 %all-gather.19.cloned.1.call-start = ((), (), s32[]{:S(2)}) async-start(), calls=%async_computation.4 | async-start | bytes 1310720 | tf_op jit(solution)/shard_map/all_gather | solution.py:57
  40.0 143.1 %copy-start.3 = (bf16[256,2048]{1,0:T(8,128)(2,1)S(1)}, bf16[256,2048]{1,0:T(8,128)(2,1)}, u32[]{:S(2)}) copy-start(bf16[256,2048]{1,0:T(8,128)(2,1)} %all-gather.11.cloned.1.call-done) | copy-start | bytes 3145732
  90.0 170.4 %copy-start = (bf16[256,512]{1,0:T(8,128)(2,1)S(1)}, bf16[256,512]{1,0:T(8,128)(2,1)}, u32[]{:S(2)}) copy-start(bf16[256,512]{1,0:T(8,128)(2,1)} %param.8) | copy-start | bytes 786436
  137.9 45.2 %collective-permute-start = (bf16[2,512]{1,0:T(2,128)(2,1)S(1)}, bf16[2,512]{1,0:T(2,128)(2,1)S(1)}, u32[]{:S(2)}, u32[]{:S(2)}) collective-permute-start(bf16[2,512]{1,0:T(2,128)(2,1)S(1)} %slice.135), channel_id=1, source_target_pairs={{0,4},{4,8},{8,12},{1,5},{5,9},{9,13},{2,6},{6,10},{10,14},{3,7},{... | collective-permute-start | bytes 6152 | tf_op jit(solution)/shard_map/ppermute | solution.py:15
  186.2 105.0 %all-gather.23.cloned.1.call-start = ((), (), s32[]{:S(2)}) async-start(), calls=%async_computation.6 | async-start | bytes 1310720 | tf_op jit(solution)/shard_map/all_gather | solution.py:36
  263.7 68.4 %all-gather.25.cloned.1.call-start = ((), (), s32[]{:S(2)}) async-start(), calls=%async_computation.7 | async-start | bytes 1310720 | tf_op jit(solution)/shard_map/all_gather | solution.py:57
  291.2 7.5 %copy-start.5 = (bf16[256,2048]{1,0:T(8,128)(2,1)S(1)}, bf16[256,2048]{1,0:T(8,128)(2,1)}, u32[]{:S(2)}) copy-start(bf16[256,2048]{1,0:T(8,128)(2,1)} %all-gather.23.cloned.1.call-done) | copy-start | bytes 3145732
  296.6 2.1 collective-permute-start.1
  301.8 61.2 %all-gather.27.cloned.1.call-start = ((), (), s32[]{:S(2)}) async-start(), calls=%async_computation.8 | async-start | bytes 1310720 | tf_op jit(solution)/shard_map/all_gather | solution.py:36
  335.5 68.4 %all-gather.29.cloned.1.call-start = ((), (), s32[]{:S(2)}) async-start(), calls=%async_computation.9 | async-start | bytes 1310720 | tf_op jit(solution)/shard_map/all_gather | solution.py:57
  363.0 7.5 %copy-start.4 = (bf16[256,2048]{1,0:T(8,128)(2,1)S(1)}, bf16[256,2048]{1,0:T(8,128)(2,1)}, u32[]{:S(2)}) copy-start(bf16[256,2048]{1,0:T(8,128)(2,1)} %all-gather.27.cloned.1.call-done) | copy-start | bytes 3145732
  368.4 48.5 %copy-start.2 = (f32[512]{0:T(512)S(1)}, f32[512]{0:T(512)}, u32[]{:S(2)}) copy-start(f32[512]{0:T(512)} %param.15) | copy-start | bytes 6148
  368.4 2.1 collective-permute-start.2
Sparse Core Ops, SparseCore 0:
  9.2 30.7 all-gather.10
  41.6 45.7 all-gather.16
  88.9 46.3 all-gather.14
  136.7 46.3 all-gather.12
  184.5 46.3 all-gather.20
  232.3 27.9 all-gather.18
  263.8 27.3 all-gather.22
  302.0 30.1 all-gather.24
  335.6 27.3 all-gather.26
  373.8 30.1 all-gather.28
where the time goes:
time: 425 us
  waiting for transfers between devices  323 us (76%)
  blocking collectives  44.2 us (10%)
  matrix products  34.6 us (8%)
  between operations  13.7 us (3%)
  starting transfers between devices  5.1 us (1%)
    all_gather x3, waiting for transfers between devices, shards(): spread = lax.all_gather(gated, 'tp', axis=1, tiled=True)  90 us
    all_gather x3, waiting for transfers between devices, shards(): gathered = lax.all_gather(normed, 'tp', axis=1, tiled=True)  49.1 us
    all_gather x1, waiting for transfers between devices, shards(): lax.all_gather(value_proj, 'sp', axis=1, tiled=True)  47.3 us
    all_gather x1, waiting for transfers between devices, shards(): lax.all_gather(in_gate, 'sp', axis=1, tiled=True)  45.3 us
    all_gather x1, waiting for transfers between devices, shards(): lax.all_gather(mix_proj, 'sp', axis=1, tiled=True)  44.6 us
    psum x4, blocking collectives, row_scale(): squares = lax.psum(jnp.sum(stream * stream, axis=1, keepdims=True), 'tp')  44.2 us
    all_gather x1, waiting for transfers between devices, shards(): lax.all_gather(out_gate, 'sp', axis=1, tiled=True)  43 us
    dot_general x9, matrix products, shards(): jnp.dot(gathered, weight[layer_index], preferred_element_type=jnp.float32)  25.2 us
  transfers between devices with their start and end apart: 13, of which 12 were waited for; matrix products, arithmetic and copies ran while one was open for 2% of the time, Pallas kernels for 0%

commit v1 on v0

--- a/solution.py
+++ b/solution.py
@@ -16,7 +16,9 @@
 
 
 def row_scale(stream):
-    squares = lax.psum(jnp.sum(stream * stream, axis=1, keepdims=True), "tp")
+    x = jnp.sum(stream * stream, axis=1, keepdims=True)
+    shards_2 = lax.all_gather(x, "tp")
+    squares = jnp.sum(shards_2, axis=0)
     return lax.rsqrt(squares / D + epsilon)
 
 

time: 425 us -> 424 us (level)
    psum x4 -> x0, blocking collectives: 44.2 us -> none  [row_scale(): squares = lax.psum(jnp.sum(stream * stream, axis=1, keepdims=True), 'tp')]
    all_gather x0 -> x4, blocking collectives: none -> 40.8 us  [row_scale(): shards_2 = lax.all_gather(x, 'tp')]
where the time goes in v1:
time: 424 us
  waiting for transfers between devices  326 us (77%)
  blocking collectives  40.8 us (10%)
  matrix products  34.6 us (8%)
  between operations  13.7 us (3%)
  starting transfers between devices  5.1 us (1%)
    all_gather x3, waiting for transfers between devices, shards(): spread = lax.all_gather(gated, 'tp', axis=1, tiled=True)  90 us
    all_gather x3, waiting for transfers between devices, shards(): gathered = lax.all_gather(normed, 'tp', axis=1, tiled=True)  51.6 us
    all_gather x1, waiting for transfers between devices, shards(): lax.all_gather(value_proj, 'sp', axis=1, tiled=True)  47.3 us
    all_gather x1, waiting for transfers between devices, shards(): lax.all_gather(in_gate, 'sp', axis=1, tiled=True)  45.3 us
    all_gather x1, waiting for transfers between devices, shards(): lax.all_gather(mix_proj, 'sp', axis=1, tiled=True)  44.6 us
    all_gather x1, waiting for transfers between devices, shards(): lax.all_gather(out_gate, 'sp', axis=1, tiled=True)  43 us
    all_gather x4, blocking collectives, row_scale(): shards_2 = lax.all_gather(x, 'tp')  40.8 us
    dot_general x9, matrix products, shards(): jnp.dot(gathered, weight[layer_index], preferred_element_type=jnp.float32)  25.2 us
  transfers between devices with their start and end apart: 13, of which 12 were waited for; matrix products, arithmetic and copies ran while one was open for 2% of the time, Pallas kernels for 0%

profile of v1, /device:TPU:0, one launch (start us, length us, event | category | flops | bytes accessed | tf_op | source)
XLA Modules:
  0.0 423.7 jit_solution(2897231548069800875)
XLA Ops:
  6.5 0.8 fusion.60
  7.4 1.7 fusion.55
  9.1 0.0 all-gather.19.cloned.1.call-update
  9.1 0.0 all-gather.25.cloned.1.call-start
  9.2 0.7 all-gather.25.cloned.1.call-update
  9.9 0.0 all-gather.23.cloned.1.call-start
  9.9 0.7 all-gather.23.cloned.1.call-update
  10.6 0.0 all-gather.21.cloned.1.call-start
  10.7 0.5 all-gather.21.cloned.1.call-update
  11.2 0.0 all-gather.29.cloned.1.call-start
  11.2 0.5 all-gather.29.cloned.1.call-update
  11.8 0.0 all-gather.27.cloned.1.call-start
  11.8 12.7 %all-gather.4 = f32[4,1,256]{2,1,0:T(1,128)S(1)} all-gather(f32[1,1,256]{2,1,0:T(1,128)S(1)} %bitcast.155), channel_id=2, replica_groups=mesh['grp'=2,'sp'=4,'tp'=4] {'tp'}, dimensions={0}, use_global_device_ids=true | all-gather | bytes 5120 | tf_op jit(solution)/shard_map/all_gather | solution.py:20
  24.5 15.4 %all-gather.19.cloned.1.call-done = bf16[256,2048]{1,0:T(8,128)(2,1)} async-done(((bf16[256,512]{1,0:T(8,128)(2,1)}), bf16[256,2048]{1,0:T(8,128)(2,1)}) %all-gather.19.cloned.1.call-update) | async-done | bytes 1048592 | tf_op jit(solution)/shard_map/all_gather | solution.py:38
  40.0 47.3 %all-gather.25.cloned.1.call-done = bf16[3,2048,512]{2,1,0:T(8,128)(2,1)} async-done(((bf16[3,512,512]{2,1,0:T(8,128)(2,1)}), bf16[3,2048,512]{2,1,0:T(8,128)(2,1)}) %all-gather.25.cloned.1.call-update) | async-done | bytes 6291472 | tf_op jit(solution)/shard_map/all_gather | solution.py:32
  87.3 2.6 fusion.39
  89.9 45.3 %all-gather.23.cloned.1.call-done = bf16[3,2048,512]{2,1,0:T(8,128)(2,1)} async-done(((bf16[3,512,512]{2,1,0:T(8,128)(2,1)}), bf16[3,2048,512]{2,1,0:T(8,128)(2,1)}) %all-gather.23.cloned.1.call-update) | async-done | bytes 6291472 | tf_op jit(solution)/shard_map/all_gather | solution.py:31
  135.3 2.6 fusion.38
  137.9 2.2 collective-permute-start
  140.1 43.0 %all-gather.21.cloned.1.call-done = bf16[3,2048,512]{2,1,0:T(8,128)(2,1)} async-done(((bf16[3,512,512]{2,1,0:T(8,128)(2,1)}), bf16[3,2048,512]{2,1,0:T(8,128)(2,1)}) %all-gather.21.cloned.1.call-update) | async-done | bytes 6291472 | tf_op jit(solution)/shard_map/all_gather | solution.py:30
  183.1 3.1 fusion.35
  186.2 0.0 all-gather.31.cloned.1.call-start
  186.3 44.6 %all-gather.29.cloned.1.call-done = bf16[3,2048,512]{2,1,0:T(8,128)(2,1)} async-done(((bf16[3,512,512]{2,1,0:T(8,128)(2,1)}), bf16[3,2048,512]{2,1,0:T(8,128)(2,1)}) %all-gather.29.cloned.1.call-update) | async-done | bytes 6291472 | tf_op jit(solution)/shard_map/all_gather | solution.py:33
  230.9 29.4 %all-gather.27.cloned.1.call-done = bf16[256,2048]{1,0:T(8,128)(2,1)} async-done(((bf16[256,512]{1,0:T(8,128)(2,1)}), bf16[256,2048]{1,0:T(8,128)(2,1)}) %all-gather.27.cloned.1.call-update) | async-done | bytes 1048592 | tf_op jit(solution)/shard_map/all_gather | solution.py:59
  260.3 3.4 multiply_reduce_fusion.2
  263.7 0.0 all-gather.33.cloned.1.call-start
  263.7 9.4 %all-gather.5 = f32[4,1,256]{2,1,0:T(1,128)S(1)} all-gather(f32[1,1,256]{2,1,0:T(1,128)S(1)} %bitcast.168), channel_id=3, replica_groups=mesh['grp'=2,'sp'=4,'tp'=4] {'tp'}, dimensions={0}, use_global_device_ids=true | all-gather | bytes 5120 | tf_op jit(solution)/shard_map/all_gather | solution.py:20
  273.1 18.1 %all-gather.31.cloned.1.call-done = bf16[256,2048]{1,0:T(8,128)(2,1)} async-done(((bf16[256,512]{1,0:T(8,128)(2,1)}), bf16[256,2048]{1,0:T(8,128)(2,1)}) %all-gather.31.cloned.1.call-update) | async-done | bytes 1048592 | tf_op jit(solution)/shard_map/all_gather | solution.py:38
  291.2 2.7 fusion.46
  293.9 2.6 fusion.45
  296.6 1.3 collective-permute-start.1
  297.9 0.8 collective-permute-done.1
  298.7 3.1 fusion.42
  301.8 0.0 all-gather.35.cloned.1.call-start
  301.9 30.3 %all-gather.33.cloned.1.call-done = bf16[256,2048]{1,0:T(8,128)(2,1)} async-done(((bf16[256,512]{1,0:T(8,128)(2,1)}), bf16[256,2048]{1,0:T(8,128)(2,1)}) %all-gather.33.cloned.1.call-update) | async-done | bytes 1048592 | tf_op jit(solution)/shard_map/all_gather | solution.py:59
  332.1 3.3 multiply_reduce_fusion.1
  335.5 0.0 all-gather.37.cloned.1.call-start
  335.5 9.4 %all-gather.6 = f32[4,1,256]{2,1,0:T(1,128)S(1)} all-gather(f32[1,1,256]{2,1,0:T(1,128)S(1)} %bitcast.167), channel_id=4, replica_groups=mesh['grp'=2,'sp'=4,'tp'=4] {'tp'}, dimensions={0}, use_global_device_ids=true | all-gather | bytes 5120 | tf_op jit(solution)/shard_map/all_gather | solution.py:20
  344.9 18.1 %all-gather.35.cloned.1.call-done = bf16[256,2048]{1,0:T(8,128)(2,1)} async-done(((bf16[256,512]{1,0:T(8,128)(2,1)}), bf16[256,2048]{1,0:T(8,128)(2,1)}) %all-gather.35.cloned.1.call-update) | async-done | bytes 1048592 | tf_op jit(solution)/shard_map/all_gather | solution.py:38
  363.0 2.7 fusion.53
  365.7 2.6 fusion.52
  368.4 1.3 collective-permute-start.2
  369.7 0.8 collective-permute-done.2
  370.5 3.1 fusion.49
  373.6 30.3 %all-gather.37.cloned.1.call-done = bf16[256,2048]{1,0:T(8,128)(2,1)} async-done(((bf16[256,512]{1,0:T(8,128)(2,1)}), bf16[256,2048]{1,0:T(8,128)(2,1)}) %all-gather.37.cloned.1.call-update) | async-done | bytes 1048592 | tf_op jit(solution)/shard_map/all_gather | solution.py:59
  403.9 2.7 multiply_reduce_fusion
  406.6 9.4 %all-gather.7 = f32[4,1,256]{2,1,0:T(1,128)S(1)} all-gather(f32[1,1,256]{2,1,0:T(1,128)S(1)} %bitcast.169), channel_id=5, replica_groups=mesh['grp'=2,'sp'=4,'tp'=4] {'tp'}, dimensions={0}, use_global_device_ids=true | all-gather | bytes 5120 | tf_op jit(solution)/shard_map/all_gather | solution.py:20
  416.0 0.8 multiply_convert_fusion
  (31 shorter events, 0.3 us)
Async XLA Ops:
  6.5 33.4 %all-gather.19.cloned.1.call-start = ((), (), s32[]{:S(2)}) async-start(), calls=%async_computation | async-start | bytes 1310720 | tf_op jit(solution)/shard_map/all_gather | solution.py:38
  9.1 78.2 %all-gather.25.cloned.1.call-start = ((), (), s32[]{:S(2)}) async-start(), calls=%async_computation.3 | async-start | bytes 7864320 | tf_op jit(solution)/shard_map/all_gather | solution.py:32
  9.9 125.4 %all-gather.23.cloned.1.call-start = ((), (), s32[]{:S(2)}) async-start(), calls=%async_computation.2 | async-start | bytes 7864320 | tf_op jit(solution)/shard_map/all_gather | solution.py:31
  10.6 129.5 %copy-start.1 = (f32[3,3,512]{2,1,0:T(4,128)S(1)}, f32[3,3,512]{2,1,0:T(4,128)}, u32[]{:S(2)}) copy-start(f32[3,3,512]{2,1,0:T(4,128)} %param.13) | copy-start | bytes 55300
  10.6 172.5 %all-gather.21.cloned.1.call-start = ((), (), s32[]{:S(2)}) async-start(), calls=%async_computation.1 | async-start | bytes 7864320 | tf_op jit(solution)/shard_map/all_gather | solution.py:30
  11.2 219.7 %all-gather.29.cloned.1.call-start = ((), (), s32[]{:S(2)}) async-start(), calls=%async_computation.5 | async-start | bytes 7864320 | tf_op jit(solution)/shard_map/all_gather | solution.py:33
  11.8 248.5 %all-gather.27.cloned.1.call-start = ((), (), s32[]{:S(2)}) async-start(), calls=%async_computation.4 | async-start | bytes 1310720 | tf_op jit(solution)/shard_map/all_gather | solution.py:59
  40.0 143.1 %copy-start.3 = (bf16[256,2048]{1,0:T(8,128)(2,1)S(1)}, bf16[256,2048]{1,0:T(8,128)(2,1)}, u32[]{:S(2)}) copy-start(bf16[256,2048]{1,0:T(8,128)(2,1)} %all-gather.19.cloned.1.call-done) | copy-start | bytes 3145732
  89.9 170.4 %copy-start = (bf16[256,512]{1,0:T(8,128)(2,1)S(1)}, bf16[256,512]{1,0:T(8,128)(2,1)}, u32[]{:S(2)}) copy-start(bf16[256,512]{1,0:T(8,128)(2,1)} %param.8) | copy-start | bytes 786436
  137.9 45.2 %collective-permute-start = (bf16[2,512]{1,0:T(2,128)(2,1)S(1)}, bf16[2,512]{1,0:T(2,128)(2,1)S(1)}, u32[]{:S(2)}, u32[]{:S(2)}) collective-permute-start(bf16[2,512]{1,0:T(2,128)(2,1)S(1)} %slice.135), channel_id=1, source_target_pairs={{0,4},{4,8},{8,12},{1,5},{5,9},{9,13},{2,6},{6,10},{10,14},{3,7},{... | collective-permute-start | bytes 6152 | tf_op jit(solution)/shard_map/ppermute | solution.py:15
  186.2 105.0 %all-gather.31.cloned.1.call-start = ((), (), s32[]{:S(2)}) async-start(), calls=%async_computation.6 | async-start | bytes 1310720 | tf_op jit(solution)/shard_map/all_gather | solution.py:38
  263.7 68.4 %all-gather.33.cloned.1.call-start = ((), (), s32[]{:S(2)}) async-start(), calls=%async_computation.7 | async-start | bytes 1310720 | tf_op jit(solution)/shard_map/all_gather | solution.py:59
  291.2 7.5 %copy-start.5 = (bf16[256,2048]{1,0:T(8,128)(2,1)S(1)}, bf16[256,2048]{1,0:T(8,128)(2,1)}, u32[]{:S(2)}) copy-start(bf16[256,2048]{1,0:T(8,128)(2,1)} %all-gather.31.cloned.1.call-done) | copy-start | bytes 3145732
  296.6 2.1 collective-permute-start.1
  301.8 61.2 %all-gather.35.cloned.1.call-start = ((), (), s32[]{:S(2)}) async-start(), calls=%async_computation.8 | async-start | bytes 1310720 | tf_op jit(solution)/shard_map/all_gather | solution.py:38
  335.5 68.4 %all-gather.37.cloned.1.call-start = ((), (), s32[]{:S(2)}) async-start(), calls=%async_computation.9 | async-start | bytes 1310720 | tf_op jit(solution)/shard_map/all_gather | solution.py:59
  363.0 7.5 %copy-start.4 = (bf16[256,2048]{1,0:T(8,128)(2,1)S(1)}, bf16[256,2048]{1,0:T(8,128)(2,1)}, u32[]{:S(2)}) copy-start(bf16[256,2048]{1,0:T(8,128)(2,1)} %all-gather.35.cloned.1.call-done) | copy-start | bytes 3145732
  368.3 47.7 %copy-start.2 = (f32[512]{0:T(512)S(1)}, f32[512]{0:T(512)}, u32[]{:S(2)}) copy-start(f32[512]{0:T(512)} %param.15) | copy-start | bytes 6148
  368.4 2.1 collective-permute-start.2
Sparse Core Ops, SparseCore 0:
  9.2 30.7 all-gather.18
  41.5 45.7 all-gather.24
  88.9 46.3 all-gather.22
  136.7 46.3 all-gather.20
  184.5 46.3 all-gather.28
  232.3 27.9 all-gather.26
  263.8 27.3 all-gather.30
  301.9 30.1 all-gather.32
  335.6 27.3 all-gather.34
  373.7 30.1 all-gather.36
